TPU v7x, 32 devices: a whole 2x2x4 slice. The times are simulated.
32 devices in a mesh: sp: 8 (over z, y), tp: 4 (over x, core).
Axes of the slice: x: 2, y: 2, z: 4, core: 2. Of those that a mesh axis runs over, the one named last changes fastest.
Arguments:
- tokens: bfloat16 [4096, 2048], P('sp', 'tp'), may hold values from -64 to 64
- conv_input: bfloat16 [2048, 1024], P(None, 'tp'), may hold values from -0.125 to 0.125
- conv_inner: bfloat16 [2048, 1024], P(None, 'tp'), may hold values from -0.125 to 0.125
- conv_outer: bfloat16 [2048, 1024], P(None, 'tp'), may hold values from -0.125 to 0.125
- conv_gate: bfloat16 [2048, 1024], P(None, 'tp'), may hold values from -0.125 to 0.125
- conv_taps: bfloat16 [3, 1024], P(None, 'tp'), may hold values from -3.5 to 3.5
- query_proj: bfloat16 [2048, 1536], P(None, 'tp'), may hold values from -8 to 8
- latent_proj: bfloat16 [2048, 256], replicated, may hold values from -1 to 1
- rope_proj: bfloat16 [2048, 32], replicated, may hold values from -0.125 to 0.125
- latent_gain: float32 [256], replicated, may hold values from 0.1 to 1.9
- key_up: bfloat16 [256, 1024], P(None, 'tp'), may hold values from -2 to 2
- value_up: bfloat16 [256, 1024], P(None, 'tp'), may hold values from -0.375 to 0.375
- attn_gate: bfloat16 [2048, 1024], P(None, 'tp'), may hold values from -0.125 to 0.125
- conv_down: bfloat16 [1024, 2048], P('tp'), may hold values from -0.1875 to 0.1875
- attn_down: bfloat16 [1024, 2048], P('tp'), may hold values from -0.75 to 0.75
Outputs:
- layer_out: bfloat16 [4096, 2048], P(('sp', 'tp'))
All inputs are finite; a program needn't handle non-finite values.
Results may differ from a plain program's by a relative error of at most 0.014.
Values may be sent and summed in bfloat16 or wider, within the bound.
A program may use at most 128 MiB of HBM per device.

v0:
```python
import jax
import jax.numpy as jnp
from jax import lax
from jax.sharding import PartitionSpec as P

NOPE = 64
ROPE = 32
VDIM = 64
GRID_W = 64
rms_eps = 1e-06
rope_theta = 10000.0


def with_halo(cells, sides, width):
    for axis, dim in sides:
        count = lax.axis_size(axis)
        ends = count - 1
        head = lax.slice_in_dim(cells, 0, width, axis=dim)
        tail = lax.slice_in_dim(cells, cells.shape[dim] - width, cells.shape[dim], axis=dim)
        cells = jnp.concatenate(
            [
                lax.ppermute(tail, axis, [(i, (i + 1) % count) for i in range(ends)]),
                cells,
                lax.ppermute(head, axis, [((i + 1) % count, i) for i in range(ends)]),
            ],
            axis=dim,
        )
    return cells


def rounded(values):
    return lax.optimization_barrier(values.astype(jnp.bfloat16))


def axial_tables(positions, rope_width, grid_width):
    quarter = rope_width // 4
    frequency = rope_theta ** (-jnp.arange(quarter, dtype=jnp.float32) * 2.0 / (rope_width // 2))
    grid_row = (positions // grid_width).astype(jnp.float32)
    grid_col = (positions % grid_width).astype(jnp.float32)
    row_angle = grid_row[:, None] * frequency[None, :]
    col_angle = grid_col[:, None] * frequency[None, :]
    return (jnp.cos(row_angle), jnp.sin(row_angle), jnp.cos(col_angle), jnp.sin(col_angle))


def turn_half(vector, cos_table, sin_table):
    half_width = vector.shape[-1] // 2
    leading = vector[..., :half_width]
    trailing = vector[..., half_width:]
    return jnp.concatenate(
        [leading * cos_table - trailing * sin_table, trailing * cos_table + leading * sin_table],
        axis=-1,
    )


def axial_turn(vector, tables):
    half_width = vector.shape[-1] // 2
    return jnp.concatenate(
        [
            turn_half(vector[..., :half_width], tables[0], tables[1]),
            turn_half(vector[..., half_width:], tables[2], tables[3]),
        ],
        axis=-1,
    )


def on_device(
    tokens,
    conv_input,
    conv_inner,
    conv_outer,
    conv_gate,
    conv_taps,
    query_proj,
    latent_proj,
    rope_proj,
    latent_gain,
    key_up,
    value_up,
    attn_gate,
    conv_down,
    attn_down,
):
    tok_rows = tokens.shape[0]
    model_width = query_proj.shape[0]
    local_heads = key_up.shape[1] // NOPE
    in_weights = (
        conv_input,
        conv_inner,
        conv_outer,
        conv_gate,
        query_proj,
        latent_proj,
        rope_proj,
        attn_gate,
    )
    widened = tokens.astype(jnp.float32)
    squares = lax.psum(jnp.sum(widened * widened, axis=1), "tp")
    shard_piece = lax.all_gather(tokens, "tp", axis=1, tiled=True)
    new_terms = tuple(
        (jnp.dot(shard_piece, matrix, preferred_element_type=jnp.float32) for matrix in in_weights)
    )
    projected = tuple((right_sum for right_sum in new_terms))
    row_scale = lax.rsqrt(squares / model_width + rms_eps)[:, None]
    value_in, inner_in, outer_in, gate_in, queries, latent, rope_in, gate_attn = tuple(
        (proj_term * row_scale for proj_term in projected)
    )
    conv_product = (
        rounded(inner_in).astype(jnp.float32) * rounded(value_in).astype(jnp.float32)
    ).astype(jnp.bfloat16)
    padded = with_halo(conv_product, (("sp", 0),), 1).astype(jnp.float32)
    tap_weights = conv_taps.astype(jnp.float32)
    conv_mixed = (
        padded[:-2] * tap_weights[0] + padded[1:-1] * tap_weights[1] + padded[2:] * tap_weights[2]
    )
    conv_out = (
        jax.nn.silu(rounded(gate_in).astype(jnp.float32))
        * rounded(outer_in).astype(jnp.float32)
        * conv_mixed
    ).astype(jnp.bfloat16)
    positions = lax.axis_index("sp") * tok_rows + jnp.arange(tok_rows, dtype=jnp.int32)
    tables = axial_tables(positions, ROPE, GRID_W)
    queries = queries.reshape(tok_rows, local_heads, NOPE + ROPE)
    query_nope = queries[..., :NOPE].astype(jnp.bfloat16)
    query_rope = axial_turn(
        queries[..., NOPE:], tuple((grid_table[:, None, :] for grid_table in tables))
    ).astype(jnp.bfloat16)
    latent = (
        latent * lax.rsqrt(jnp.mean(latent * latent, axis=1, keepdims=True) + rms_eps) * latent_gain
    ).astype(jnp.bfloat16)
    key_rope = axial_turn(rope_in, tables).astype(jnp.bfloat16)
    score_scale = (NOPE + ROPE) ** (-0.5)
    initial = (
        jnp.full((tok_rows, local_heads), -jnp.inf, jnp.float32),
        jnp.zeros((tok_rows, local_heads), jnp.float32),
        jnp.zeros((tok_rows, local_heads, VDIM), jnp.float32),
    )
    latent_piece = lax.all_gather(latent, "sp", axis=0, tiled=True)
    rope_piece = lax.all_gather(key_rope, "sp", axis=0, tiled=True)
    key_count = latent_piece.shape[0]
    span_rows = key_count
    while span_rows > 1024 and span_rows % 2 == 0:
        span_rows = span_rows // 2

    def one_span(state_now, span_start):
        latent_span = lax.dynamic_slice_in_dim(latent_piece, span_start, span_rows, 0)
        rope_span = lax.dynamic_slice_in_dim(rope_piece, span_start, span_rows, 0)
        key_nope = (
            jnp.dot(latent_span, key_up, preferred_element_type=jnp.float32)
            .astype(jnp.bfloat16)
            .reshape(span_rows, local_heads, NOPE)
        )
        key_values = (
            jnp.dot(latent_span, value_up, preferred_element_type=jnp.float32)
            .astype(jnp.bfloat16)
            .reshape(span_rows, local_heads, VDIM)
        )
        scores = jnp.einsum(
            "qhd,khd->qhk", query_nope, key_nope, preferred_element_type=jnp.float32
        )
        scores = (
            scores
            + jnp.einsum("qhd,kd->qhk", query_rope, rope_span, preferred_element_type=jnp.float32)
        ) * score_scale
        row_top, weight_total, weighted = state_now
        new_top = jnp.maximum(row_top, jnp.max(scores, axis=2))
        weights = jnp.exp(scores - new_top[:, :, None])
        shrink = jnp.exp(row_top - new_top)
        weight_total = weight_total * shrink + jnp.sum(weights, axis=2)
        weighted = weighted * shrink[:, :, None] + jnp.einsum(
            "qhk,khd->qhd",
            weights.astype(jnp.bfloat16),
            key_values,
            preferred_element_type=jnp.float32,
        )
        return ((new_top, weight_total, weighted), None)

    span_starts = jnp.arange(key_count // span_rows, dtype=jnp.int32) * span_rows
    gathered_state = lax.scan(one_span, initial, span_starts)[0]
    attended = (gathered_state[2] / gathered_state[1][:, :, None]).reshape(
        tok_rows, local_heads * VDIM
    )
    attn_out = (jax.nn.silu(rounded(gate_attn).astype(jnp.float32)) * attended).astype(jnp.bfloat16)
    return lax.psum_scatter(
        (
            jnp.dot(conv_out, conv_down, preferred_element_type=jnp.float32)
            + jnp.dot(attn_out, attn_down, preferred_element_type=jnp.float32)
        ).astype(jnp.bfloat16),
        "tp",
        scatter_dimension=0,
        tiled=True,
    )


def solution(mesh):
    placed = (
        P("sp", "tp"),
        P(None, "tp"),
        P(None, "tp"),
        P(None, "tp"),
        P(None, "tp"),
        P(None, "tp"),
        P(None, "tp"),
        P(),
        P(),
        P(),
        P(None, "tp"),
        P(None, "tp"),
        P(None, "tp"),
        P("tp", None),
        P("tp", None),
    )
    return jax.shard_map(
        on_device, mesh=mesh, in_specs=placed, out_specs=P(("sp", "tp"), None), check_vma=False
    )
```

profile of v0, /device:TPU:0, one launch (start us, length us, event | category | flops | bytes accessed | tf_op | source)
XLA Modules:
  0.0 174.0 jit_solution(3789378869783381804)
XLA Ops:
  8.6 8.4 %psum.7 = f32[512]{0:T(512)S(1)} all-reduce(f32[512]{0:T(512)S(1)} %multiply_reduce_fusion), channel_id=1, replica_groups=mesh['sp'=8,'tp'=4] {'tp'}, use_global_device_ids=true, to_apply=%region_1.0 | all-reduce | flops 512 | bytes 4096 | tf_op jit(solution)/shard_map/psum | solution.py:97
  17.8 16.4 %all-gather.3.cloned.1.call-done = bf16[512,2048]{1,0:T(8,128)(2,1)} async-done(((bf16[512,512]{1,0:T(8,128)(2,1)}), bf16[512,2048]{1,0:T(8,128)(2,1)}) %all-gather.3.cloned.1.call-update) | async-done | bytes 2097168 | tf_op jit(solution)/shard_map/all_gather | solution.py:98
  34.2 2.6 %multiply_reduce_fusion.1 = (f32[512]{0:T(512)S(1)}, f32[512,256]{1,0:T(8,128)S(1)}) fusion(f32[512]{0:T(512)S(1)} %add_rsqrt_fusion.1, bf16[512,2048]{1,0:T(8,128)(2,1)} %all-gather.3.cloned.1.call-done, bf16[2048,256]{1,0:T(8,128)(2,1)} %param.24), kind=kOutput, calls=%fused_computation.58 | convolution fusion | flops 537263616 | bytes 3674112 | tf_op jit(solution)/shard_map/dot_general | solution.py:100
  37.8 2.7 %fusion.22 = bf16[512,256]{1,0:T(8,128)(2,1)S(1)} fusion(bf16[512,2048]{1,0:T(8,128)(2,1)} %all-gather.3.cloned.1.call-done, bf16[2048,256]{1,0:T(8,128)(2,1)} %param.19, f32[512]{0:T(512)S(1)} %add_rsqrt_fusion.1), kind=kOutput, calls=%fused_computation.33 | convolution fusion | flops 537133056 | bytes 3409920 | tf_op jit(solution)/shard_map/dot_general | solution.py:100
  41.4 3.4 %collective-permute-start = (bf16[1,256]{1,0:T(2,128)(2,1)S(1)}, bf16[1,256]{1,0:T(2,128)(2,1)S(1)}, u32[]{:S(2)}, u32[]{:S(2)}) collective-permute-start(bf16[1,256]{1,0:T(2,128)(2,1)S(1)} %get-tuple-element.133), channel_id=1, source_target_pairs={{0,4},{4,8},{8,12},{12,16},{16,20},{20,24},{24,28},{1,5},{5,9},{9,... | collective-permute-start | bytes 1544 | tf_op jit(solution)/shard_map/ppermute | solution.py:22
  51.5 34.1 %all_gather.11 = bf16[4096,32]{0,1:T(8,128)(2,1)S(1)} all-gather(bf16[512,32]{0,1:T(8,128)(2,1)S(1)} %pad_maximum_fusion.1), channel_id=1, replica_groups=mesh['sp'=8,'tp'=4] {'sp'}, dimensions={0}, use_global_device_ids=true | all-gather | bytes 294912 | tf_op jit(solution)/shard_map/all_gather | solution.py:138
  85.8 2.9 %fusion.38 = f32[512,2048]{1,0:T(8,128)} fusion(bf16[256,2048]{1,0:T(8,128)(2,1)S(1)} %copy-done.4, f32[514,256]{1,0:T(8,128)S(1)} %maximum_convert_fusion, bf16[512,256]{1,0:T(8,128)(2,1)S(1)} %fusion.21, bf16[512,256]{1,0:T(8,128)(2,1)S(1)} %fusion.20, f32[256]{0:T(256)S(1)} %bitcast.76, f32[256]{0:T(256)S(1)} %bitcast.75, f32[256]{0:T(256)S(1)} %bitcast.74), kind=kOutput, calls=%fused_computation.63 | convolution fusion | flops 538705920 | bytes 7343104 | tf_op jit(solution)/shard_map/dot_general | solution.py:185
  89.5 43.0 %while.15 = (s32[]{:T(128)}, f32[512,4]{0,1:T(4,128)S(1)}, f32[512,4]{0,1:T(4,128)S(1)}, f32[512,4,64]{0,2,1:T(8,128)S(1)}, s32[4]{0:T(128)S(1)}, /*index=5*/bf1...) while((s32[]{:T(128)}, f32[512,4]{0,1:T(4,128)S(1)}, ...), condition=%wide.region_6.7_spmd.clone, body=%wide.region_3.6_spmd.clone.sunk | while | flops 955131904 | bytes 46989520 | solution.py:178
  93.4 1.4 convolution_convert_fusion.4
  96.1 1.4 fusion.105
  98.7 1.5 fusion.108
  102.8 1.4 convolution_convert_fusion.5
  104.2 1.4 convolution_convert_fusion.4
  106.9 1.4 fusion.105
  109.5 1.5 fusion.108
  113.5 1.4 convolution_convert_fusion.5
  114.9 1.4 convolution_convert_fusion.4
  117.6 1.4 fusion.105
  120.2 1.5 fusion.108
  125.7 1.4 convolution_convert_fusion.4
  128.4 1.4 fusion.105
  131.0 1.5 fusion.108
  132.8 4.6 %add_convert_fusion = bf16[512,2048]{1,0:T(8,128)(2,1)} fusion(f32[512,2048]{1,0:T(8,128)} %fusion.38, bf16[256,2048]{1,0:T(8,128)(2,1)} %param.31, f32[512,256]{1,0:T(8,128)S(1)} %copy.21, bf16[512,256]{1,0:T(8,128)(2,1)S(1)} %fusion.24), kind=kOutput, calls=%fused_computation.23 | convolution fusion | flops 539885568 | bytes 8126464 | tf_op jit(solution)/shard_map/dot_general | solution.py:186
  137.4 30.1 %reduce-scatter.2.cloned.1.call-done = bf16[128,2048]{1,0:T(8,128)(2,1)} async-done(((bf16[512,2048]{1,0:T(8,128)(2,1)}), bf16[128,2048]{1,0:T(8,128)(2,1)}) %reduce-scatter.2.cloned.1.call-update) | async-done | bytes 524304 | tf_op jit(solution)/shard_map/reduce_scatter | solution.py:183
  (85 shorter events, 27.2 us)
Async XLA Ops:
  6.5 40.5 %copy-start = (bf16[2048,384]{1,0:T(8,128)(2,1)S(1)}, bf16[2048,384]{1,0:T(8,128)(2,1)}, u32[]{:S(2)}) copy-start(bf16[2048,384]{1,0:T(8,128)(2,1)} %param.23) | copy-start | bytes 4718596
  6.5 27.7 %all-gather.3.cloned.1.call-start = ((), (), s32[]{:S(2)}) async-start(), calls=%async_computation.1 | async-start | bytes 2621440 | tf_op jit(solution)/shard_map/all_gather | solution.py:98
  7.3 82.2 %all-gather.5.cloned.1.call-start = ((), (), s32[]{:S(2)}) async-start(), calls=%async_computation.2 | async-start | bytes 2359296 | tf_op jit(solution)/shard_map/all_gather | solution.py:137
  17.8 19.1 %copy-start.6 = (f32[256]{0:T(256)S(1)}, f32[256]{0:T(256)}, u32[]{:S(2)}) copy-start(f32[256]{0:T(256)} %param.26) | copy-start | bytes 3076
  37.7 129.7 %reduce-scatter.2.cloned.1.call-start = ((), (), s32[]{:S(2)}) async-start(), calls=%async_computation.3 | async-start | bytes 2621440 | tf_op jit(solution)/shard_map/reduce_scatter | solution.py:183
  37.8 2.7 %copy-start.3 = (bf16[512,2048]{1,0:T(8,128)(2,1)S(1)}, bf16[512,2048]{1,0:T(8,128)(2,1)}, u32[]{:S(2)}) copy-start(bf16[512,2048]{1,0:T(8,128)(2,1)} %all-gather.3.cloned.1.call-done) | copy-start | bytes 6291460
  37.8 2.8 %copy-start.7 = (bf16[2048,256]{1,0:T(8,128)(2,1)S(1)}, bf16[2048,256]{1,0:T(8,128)(2,1)}, u32[]{:S(2)}) copy-start(bf16[2048,256]{1,0:T(8,128)(2,1)} %param.18) | copy-start | bytes 3145732
  40.6 5.5 %copy-start.5 = (bf16[2048,32]{0,1:T(8,128)(2,1)S(1)}, bf16[2048,32]{0,1:T(8,128)(2,1)}, u32[]{:S(2)}) copy-start(bf16[2048,32]{0,1:T(8,128)(2,1)} %param.25) | copy-start | bytes 393220
  41.4 44.3 %collective-permute-start = (bf16[1,256]{1,0:T(2,128)(2,1)S(1)}, bf16[1,256]{1,0:T(2,128)(2,1)S(1)}, u32[]{:S(2)}, u32[]{:S(2)}) collective-permute-start(bf16[1,256]{1,0:T(2,128)(2,1)S(1)} %get-tuple-element.133), channel_id=1, source_target_pairs={{0,4},{4,8},{8,12},{12,16},{16,20},{20,24},{24,28},{1,5},{5,9},{9,... | collective-permute-start | bytes 1544 | tf_op jit(solution)/shard_map/ppermute | solution.py:22
  44.8 40.9 %collective-permute-start.1 = (bf16[1,256]{1,0:T(2,128)(2,1)S(1)}, bf16[1,256]{1,0:T(2,128)(2,1)S(1)}, u32[]{:S(2)}, u32[]{:S(2)}) collective-permute-start(bf16[1,256]{1,0:T(2,128)(2,1)S(1)} %get-tuple-element.134), channel_id=1, source_target_pairs={{4,0},{8,4},{12,8},{16,12},{20,16},{24,20},{28,24},{5,1},{9,5},{13... | collective-permute-start | bytes 1544 | tf_op jit(solution)/shard_map/ppermute | solution.py:24
  47.1 1.2 copy-start.8
  48.3 1.2 copy-start.9
  49.5 1.2 copy-start.10
  51.5 34.3 %copy-start.4 = (bf16[256,2048]{1,0:T(8,128)(2,1)S(1)}, bf16[256,2048]{1,0:T(8,128)(2,1)}, u32[]{:S(2)}) copy-start(bf16[256,2048]{1,0:T(8,128)(2,1)} %param.30) | copy-start | bytes 3145732
  85.8 3.7 %copy-start.1 = (bf16[256,256]{1,0:T(8,128)(2,1)S(1)}, bf16[256,256]{1,0:T(8,128)(2,1)}, u32[]{:S(2)}) copy-start(bf16[256,256]{1,0:T(8,128)(2,1)} %param.27) | copy-start | bytes 393220
  85.8 3.7 %copy-start.2 = (bf16[256,256]{1,0:T(8,128)(2,1)S(1)}, bf16[256,256]{1,0:T(8,128)(2,1)}, u32[]{:S(2)}) copy-start(bf16[256,256]{1,0:T(8,128)(2,1)} %param.28) | copy-start | bytes 393220
Sparse Core Ops, SparseCore 0:
  8.9 25.2 all-gather.2
  37.9 51.5 all-gather.4
  137.5 29.9 reduce-scatter.1
where the time goes:
time: 175 us; the launch traced here: 174 us
  waiting for transfers between devices  48.1 us (27%)
  matrix products  45.5 us (26%)
  blocking collectives  42.5 us (24%)
  between operations  13.4 us (8%)
  loops' own time  8.05 us (5%)
  other arithmetic  7.14 us (4%)
  starting transfers between devices  4.75 us (3%)
  local copies, waits for them, and re-layouts  4.6 us (3%)
    all_gather x1, blocking collectives, on_device(): rope_piece = lax.all_gather(key_rope, 'sp', axis=0, tiled=True)  34.1 us
    reduce_scatter x1, waiting for transfers between devices, on_device(): lax.psum_scatter((jnp.dot(conv_out, conv_down, preferred_element_type=jnp...  30.1 us
    all_gather x1, waiting for transfers between devices, on_device(): shard_piece = lax.all_gather(tokens, 'tp', axis=1, tiled=True)  16.4 us
    dot_general x8, matrix products, on_device(): jnp.dot(shard_piece, matrix, preferred_element_type=jnp.float32)  9.98 us
    psum x1, blocking collectives, on_device(): squares = lax.psum(jnp.sum(widened * widened, axis=1), 'tp')  8.37 us
    another operation x1, loops' own time, on_device(): gathered_state = lax.scan(one_span, initial, span_starts)[0]  8.05 us
    dot_general x4, matrix products, one_span(): jnp.einsum('qhk,khd->qhd', weights.astype(jnp.bfloat16), key_values, pref...  5.94 us
    dot_general x4, matrix products, one_span(): jnp.einsum('qhd,kd->qhk', query_rope, rope_span, preferred_element_type=j...  5.76 us
  transfers between devices with their start and end apart: 5, of which 3 were waited for; matrix products, arithmetic and copies ran while one was open for 7% of the time, Pallas kernels for 0%

commit v1 on v0

--- a/solution.py
+++ b/solution.py
@@ -134,8 +134,11 @@
         jnp.zeros((tok_rows, local_heads), jnp.float32),
         jnp.zeros((tok_rows, local_heads, VDIM), jnp.float32),
     )
-    latent_piece = lax.all_gather(latent, "sp", axis=0, tiled=True)
-    rope_piece = lax.all_gather(key_rope, "sp", axis=0, tiled=True)
+    latent_piece, rope_piece = jnp.split(
+        lax.all_gather(jnp.concatenate([latent, key_rope], axis=1), "sp", axis=0, tiled=True),
+        [latent.shape[1]],
+        axis=1,
+    )
     key_count = latent_piece.shape[0]
     span_rows = key_count
     while span_rows > 1024 and span_rows % 2 == 0:

time: 175 us -> 196 us (1.12)
  waiting for transfers between devices: 48.1 us -> 90.6 us
  blocking collectives: 42.5 us -> 8.37 us
  local copies, waits for them, and re-layouts: 4.6 us -> 12.1 us
  matrix products: 45.5 us -> 50.8 us
    all_gather x1, waiting for transfers between devices: 0.82 us -> 42.6 us  [on_device(): lax.all_gather(jnp.concatenate([latent, key_rope], axis=1), 'sp', axis=0,...]
    all_gather x1 -> x0, blocking collectives: 34.1 us -> none  [on_device(): rope_piece = lax.all_gather(key_rope, 'sp', axis=0, tiled=True)]
    split x0 -> x3, local copies, waits for them, and re-layouts: none -> 4.39 us  [on_device(): jnp.split(lax.all_gather(jnp.concatenate([latent, key_rope], axis=1), 'sp...]
    dot_general x4, matrix products: 5.76 us -> 9.21 us  [one_span(): jnp.einsum('qhd,kd->qhk', query_rope, rope_span, preferred_element_type=j...]
    unnamed x22 -> x31, local copies, waits for them, and re-layouts: 1.2 us -> 3.32 us
  transfers between devices with their start and end apart: 5 -> 5, of which waited for: 3 -> 3; matrix products, arithmetic and copies ran while one was open for 7% -> 6% of each run, Pallas kernels for 0% -> 0%
where the time goes in v1:
time: 196 us; the launch traced here: 195 us
  waiting for transfers between devices  90.6 us (46%)
  matrix products  50.8 us (26%)
  between operations  13.5 us (7%)
  local copies, waits for them, and re-layouts  12.1 us (6%)
  blocking collectives  8.37 us (4%)
  loops' own time  7.92 us (4%)
  other arithmetic  7 us (4%)
  starting transfers between devices  5.06 us (3%)
    all_gather x1, waiting for transfers between devices, on_device(): lax.all_gather(jnp.concatenate([latent, key_rope], axis=1), 'sp', axis=0,...  42.6 us
    reduce_scatter x1, waiting for transfers between devices, on_device(): lax.psum_scatter((jnp.dot(conv_out, conv_down, preferred_element_type=jnp...  30 us
    all_gather x1, waiting for transfers between devices, on_device(): shard_piece = lax.all_gather(tokens, 'tp', axis=1, tiled=True)  17.3 us
    dot_general x8, matrix products, on_device(): jnp.dot(shard_piece, matrix, preferred_element_type=jnp.float32)  11.8 us
    dot_general x4, matrix products, one_span(): jnp.einsum('qhd,kd->qhk', query_rope, rope_span, preferred_element_type=j...  9.21 us
    psum x1, blocking collectives, on_device(): squares = lax.psum(jnp.sum(widened * widened, axis=1), 'tp')  8.37 us
    another operation x1, loops' own time, on_device(): gathered_state = lax.scan(one_span, initial, span_starts)[0]  7.92 us
    dot_general x4, matrix products, one_span(): jnp.einsum('qhk,khd->qhd', weights.astype(jnp.bfloat16), key_values, pref...  5.93 us
  transfers between devices with their start and end apart: 5, of which 3 were waited for; matrix products, arithmetic and copies ran while one was open for 6% of the time, Pallas kernels for 0%

profile of v1, /device:TPU:0, one launch (start us, length us, event | category | flops | bytes accessed | tf_op | source)
XLA Modules:
  0.0 195.2 jit_solution(8511922244954828938)
XLA Ops:
  8.5 8.4 %psum.7 = f32[512]{0:T(512)S(1)} all-reduce(f32[512]{0:T(512)S(1)} %multiply_reduce_fusion), channel_id=1, replica_groups=mesh['sp'=8,'tp'=4] {'tp'}, use_global_device_ids=true, to_apply=%region_1.0 | all-reduce | flops 512 | bytes 4096 | tf_op jit(solution)/shard_map/psum | solution.py:97
  17.0 17.3 %all-gather.3.cloned.1.call-done = bf16[512,2048]{1,0:T(8,128)(2,1)} async-done(((bf16[512,512]{1,0:T(8,128)(2,1)}), bf16[512,2048]{1,0:T(8,128)(2,1)}) %all-gather.3.cloned.1.call-update) | async-done | bytes 2097168 | tf_op jit(solution)/shard_map/all_gather | solution.py:98
  34.2 2.3 %convolution_multiply_fusion.7 = f32[512,32]{0,1:T(8,128)S(1)} fusion(bf16[512,2048]{1,0:T(8,128)(2,1)} %all-gather.3.cloned.1.call-done, bf16[2048,32]{0,1:T(8,128)(2,1)} %param.25, f32[512]{0:T(512)S(1)} %add_rsqrt_fusion.1), kind=kOutput, calls=%fused_computation.36 | convolution fusion | flops 67125248 | bytes 2295808 | tf_op jit(solution)/shard_map/dot_general | solution.py:100
  37.5 2.4 %multiply_reduce_fusion.1 = (f32[512]{0:T(512)S(1)}, f32[512,256]{1,0:T(8,128)S(1)}) fusion(f32[512]{0:T(512)S(1)} %add_rsqrt_fusion.1, bf16[512,2048]{1,0:T(8,128)(2,1)} %all-gather.3.cloned.1.call-done, bf16[2048,256]{1,0:T(8,128)(2,1)S(1)} %copy-done.8), kind=kOutput, calls=%fused_computation.58 | convolution fusion | flops 537263616 | bytes 3674112 | tf_op jit(solution)/shard_map/dot_general | solution.py:100
  41.8 2.5 %fusion.22 = bf16[512,256]{1,0:T(8,128)(2,1)S(1)} fusion(bf16[512,2048]{1,0:T(8,128)(2,1)} %all-gather.3.cloned.1.call-done, bf16[2048,256]{1,0:T(8,128)(2,1)S(1)} %copy-done.9, f32[512]{0:T(512)S(1)} %add_rsqrt_fusion.1), kind=kOutput, calls=%fused_computation.33 | convolution fusion | flops 537133056 | bytes 3409920 | tf_op jit(solution)/shard_map/dot_general | solution.py:100
  45.1 3.4 %collective-permute-start = (bf16[1,256]{1,0:T(2,128)(2,1)S(1)}, bf16[1,256]{1,0:T(2,128)(2,1)S(1)}, u32[]{:S(2)}, u32[]{:S(2)}) collective-permute-start(bf16[1,256]{1,0:T(2,128)(2,1)S(1)} %get-tuple-element.166), channel_id=1, source_target_pairs={{0,4},{4,8},{8,12},{12,16},{16,20},{20,24},{24,28},{1,5},{5,9},{9,... | collective-permute-start | bytes 1544 | tf_op jit(solution)/shard_map/ppermute | solution.py:22
  48.5 1.6 collective-permute-start.1
  52.4 1.4 fusion.24
  55.8 2.9 %fusion.38 = f32[512,2048]{1,0:T(8,128)} fusion(bf16[256,2048]{1,0:T(8,128)(2,1)S(1)} %copy-done.4, f32[514,256]{1,0:T(8,128)S(1)} %maximum_convert_fusion, bf16[512,256]{1,0:T(8,128)(2,1)S(1)} %fusion.21, bf16[512,256]{1,0:T(8,128)(2,1)S(1)} %fusion.20, f32[256]{0:T(256)S(1)} %bitcast.76, f32[256]{0:T(256)S(1)} %bitcast.75, f32[256]{0:T(256)S(1)} %bitcast.74), kind=kOutput, calls=%fused_computation.63 | convolution fusion | flops 538705920 | bytes 7343104 | tf_op jit(solution)/shard_map/dot_general | solution.py:188
  58.7 42.6 %all-gather.5.cloned.1.call-done = bf16[4096,288]{1,0:T(8,128)(2,1)} async-done(((bf16[512,288]{1,0:T(8,128)(2,1)}), bf16[4096,288]{1,0:T(8,128)(2,1)}) %all-gather.5.cloned.1.call-update) | async-done | bytes 2359312 | tf_op jit(solution)/shard_map/all_gather | solution.py:138
  103.5 3.2 %split.8 = bf16[4096,256]{1,0:T(8,128)(2,1)} slice(bf16[4096,288]{1,0:T(8,128)(2,1)} %all-gather.5.cloned.1.call-done), slice={[0:4096], [0:256]} | slice | bytes 4194304 | tf_op jit(solution)/shard_map/split | solution.py:137
  106.7 46.4 %while.15 = (s32[]{:T(128)}, f32[512,4]{0,1:T(4,128)S(1)}, f32[512,4]{0,1:T(4,128)S(1)}, f32[512,4,64]{0,2,1:T(8,128)S(1)}, s32[4]{0:T(128)S(1)}, /*index=5*/bf1...) while((s32[]{:T(128)}, f32[512,4]{0,1:T(4,128)S(1)}, ...), condition=%wide.region_6.7_spmd.clone, body=%wide.region_3.6_spmd.clone.sunk | while | flops 955131904 | bytes 46989520 | solution.py:181
  110.6 1.4 convolution_convert_fusion.4
  113.4 2.3 %fusion.105 = (f32[512,4]{0,1:T(4,128)S(1)}, f32[512,4,1024]{0,2,1:T(8,128)S(1)}) fusion(bf16[512,4,32]{0,2,1:T(8,128)(2,1)S(1)} %get-tuple-element.303, bf16[4096,32]{0,1:T(8,128)(2,1)} %get-tuple-element.302, s32[]{:T(128)S(6)} %select_n.34, f32[4,1024,512]{2,1,0:T(8,128)S(1)} %fusion.104), kind=kOutput, calls=%fused_computation.101.clone.1 | convolution fusion | flops 140507136 | bytes 16982020 | tf_op jit(solution)/shard_map/while/body/eval_jaxpr/qhd,kd->qhk/dot_general | solution.py:165
  116.8 1.5 fusion.108
  122.3 1.4 convolution_convert_fusion.4
  125.0 2.3 %fusion.105 = (f32[512,4]{0,1:T(4,128)S(1)}, f32[512,4,1024]{0,2,1:T(8,128)S(1)}) fusion(bf16[512,4,32]{0,2,1:T(8,128)(2,1)S(1)} %get-tuple-element.303, bf16[4096,32]{0,1:T(8,128)(2,1)} %get-tuple-element.302, s32[]{:T(128)S(6)} %select_n.34, f32[4,1024,512]{2,1,0:T(8,128)S(1)} %fusion.104), kind=kOutput, calls=%fused_computation.101.clone.1 | convolution fusion | flops 140507136 | bytes 16982020 | tf_op jit(solution)/shard_map/while/body/eval_jaxpr/qhd,kd->qhk/dot_general | solution.py:165
  128.5 1.5 fusion.108
  136.6 2.3 %fusion.105 = (f32[512,4]{0,1:T(4,128)S(1)}, f32[512,4,1024]{0,2,1:T(8,128)S(1)}) fusion(bf16[512,4,32]{0,2,1:T(8,128)(2,1)S(1)} %get-tuple-element.303, bf16[4096,32]{0,1:T(8,128)(2,1)} %get-tuple-element.302, s32[]{:T(128)S(6)} %select_n.34, f32[4,1024,512]{2,1,0:T(8,128)S(1)} %fusion.104), kind=kOutput, calls=%fused_computation.101.clone.1 | convolution fusion | flops 140507136 | bytes 16982020 | tf_op jit(solution)/shard_map/while/body/eval_jaxpr/qhd,kd->qhk/dot_general | solution.py:165
  140.1 1.5 fusion.108
  148.2 2.3 %fusion.105 = (f32[512,4]{0,1:T(4,128)S(1)}, f32[512,4,1024]{0,2,1:T(8,128)S(1)}) fusion(bf16[512,4,32]{0,2,1:T(8,128)(2,1)S(1)} %get-tuple-element.303, bf16[4096,32]{0,1:T(8,128)(2,1)} %get-tuple-element.302, s32[]{:T(128)S(6)} %select_n.34, f32[4,1024,512]{2,1,0:T(8,128)S(1)} %fusion.104), kind=kOutput, calls=%fused_computation.101.clone.1 | convolution fusion | flops 140507136 | bytes 16982020 | tf_op jit(solution)/shard_map/while/body/eval_jaxpr/qhd,kd->qhk/dot_general | solution.py:165
  151.6 1.5 fusion.108
  154.1 4.6 %add_convert_fusion = bf16[512,2048]{1,0:T(8,128)(2,1)} fusion(f32[512,2048]{1,0:T(8,128)} %fusion.38, bf16[256,2048]{1,0:T(8,128)(2,1)} %param.31, f32[512,256]{1,0:T(8,128)S(1)} %copy.41, bf16[512,256]{1,0:T(8,128)(2,1)S(1)} %copy-done.5), kind=kOutput, calls=%fused_computation.23 | convolution fusion | flops 539885568 | bytes 8126464 | tf_op jit(solution)/shard_map/dot_general | solution.py:189
  158.8 30.0 %reduce-scatter.2.cloned.1.call-done = bf16[128,2048]{1,0:T(8,128)(2,1)} async-done(((bf16[512,2048]{1,0:T(8,128)(2,1)}), bf16[128,2048]{1,0:T(8,128)(2,1)}) %reduce-scatter.2.cloned.1.call-update) | async-done | bytes 524304 | tf_op jit(solution)/shard_map/reduce_scatter | solution.py:186
  (100 shorter events, 33.5 us)
Async XLA Ops:
  6.5 43.5 %copy-start = (bf16[2048,384]{1,0:T(8,128)(2,1)S(1)}, bf16[2048,384]{1,0:T(8,128)(2,1)}, u32[]{:S(2)}) copy-start(bf16[2048,384]{1,0:T(8,128)(2,1)} %param.23) | copy-start | bytes 4718596
  6.5 30.9 %copy-start.8 = (bf16[2048,256]{1,0:T(8,128)(2,1)S(1)}, bf16[2048,256]{1,0:T(8,128)(2,1)}, u32[]{:S(2)}) copy-start(bf16[2048,256]{1,0:T(8,128)(2,1)} %param.24) | copy-start | bytes 3145732
  6.5 27.7 %all-gather.3.cloned.1.call-start = ((), (), s32[]{:S(2)}) async-start(), calls=%async_computation.1 | async-start | bytes 2621440 | tf_op jit(solution)/shard_map/all_gather | solution.py:98
  7.3 94.0 %all-gather.5.cloned.1.call-start = ((), (), s32[]{:S(2)}) async-start(), calls=%async_computation.2 | async-start | bytes 3538944 | tf_op jit(solution)/shard_map/all_gather | solution.py:138
  37.4 2.4 %copy-start.7 = (f32[256]{0:T(256)S(1)}, f32[256]{0:T(256)}, u32[]{:S(2)}) copy-start(f32[256]{0:T(256)} %param.26) | copy-start | bytes 3076
  39.8 1.9 copy-start.6
  39.9 1.9 copy-start.9
  41.1 147.6 %reduce-scatter.2.cloned.1.call-start = ((), (), s32[]{:S(2)}) async-start(), calls=%async_computation.3 | async-start | bytes 2621440 | tf_op jit(solution)/shard_map/reduce_scatter | solution.py:186
  41.8 2.5 %copy-start.3 = (bf16[512,2048]{1,0:T(8,128)(2,1)S(1)}, bf16[512,2048]{1,0:T(8,128)(2,1)}, u32[]{:S(2)}) copy-start(bf16[512,2048]{1,0:T(8,128)(2,1)} %all-gather.3.cloned.1.call-done) | copy-start | bytes 6291460
  41.8 2.5 %copy-start.10 = (bf16[2048,256]{1,0:T(8,128)(2,1)S(1)}, bf16[2048,256]{1,0:T(8,128)(2,1)}, u32[]{:S(2)}) copy-start(bf16[2048,256]{1,0:T(8,128)(2,1)} %param.18) | copy-start | bytes 3145732
  45.1 9.6 %collective-permute-start = (bf16[1,256]{1,0:T(2,128)(2,1)S(1)}, bf16[1,256]{1,0:T(2,128)(2,1)S(1)}, u32[]{:S(2)}, u32[]{:S(2)}) collective-permute-start(bf16[1,256]{1,0:T(2,128)(2,1)S(1)} %get-tuple-element.166), channel_id=1, source_target_pairs={{0,4},{4,8},{8,12},{12,16},{16,20},{20,24},{24,28},{1,5},{5,9},{9,... | collective-permute-start | bytes 1544 | tf_op jit(solution)/shard_map/ppermute | solution.py:22
  48.5 2.7 %copy-start.11 = (bf16[2048,256]{1,0:T(8,128)(2,1)S(1)}, bf16[2048,256]{1,0:T(8,128)(2,1)}, u32[]{:S(2)}) copy-start(bf16[2048,256]{1,0:T(8,128)(2,1)} %param.20) | copy-start | bytes 3145732
  48.5 6.2 %collective-permute-start.1 = (bf16[1,256]{1,0:T(2,128)(2,1)S(1)}, bf16[1,256]{1,0:T(2,128)(2,1)S(1)}, u32[]{:S(2)}, u32[]{:S(2)}) collective-permute-start(bf16[1,256]{1,0:T(2,128)(2,1)S(1)} %get-tuple-element.167), channel_id=1, source_target_pairs={{4,0},{8,4},{12,8},{16,12},{20,16},{24,20},{28,24},{5,1},{9,5},{13... | collective-permute-start | bytes 1544 | tf_op jit(solution)/shard_map/ppermute | solution.py:24
  51.2 1.2 copy-start.12
  52.4 1.4 copy-start.13
  54.6 1.2 copy-start.4
  101.3 1.2 slice-start
  103.5 3.2 %copy-start.1 = (bf16[256,256]{1,0:T(8,128)(2,1)S(1)}, bf16[256,256]{1,0:T(8,128)(2,1)}, u32[]{:S(2)}) copy-start(bf16[256,256]{1,0:T(8,128)(2,1)} %param.27) | copy-start | bytes 393220
  103.5 3.2 %copy-start.2 = (bf16[256,256]{1,0:T(8,128)(2,1)S(1)}, bf16[256,256]{1,0:T(8,128)(2,1)}, u32[]{:S(2)}) copy-start(bf16[256,256]{1,0:T(8,128)(2,1)} %param.28) | copy-start | bytes 393220
  103.5 3.2 %copy-start.14 = (s32[4]{0:T(128)S(1)}, s32[4]{0:T(128)}, u32[]{:S(2)}) copy-start(s32[4]{0:T(128)} %iota_multiply_fusion) | copy-start | bytes 52
  153.2 1.0 copy-start.5
Sparse Core Ops, SparseCore 0:
  8.9 25.2 all-gather.2
  41.2 60.0 all-gather.4
  158.9 29.7 reduce-scatter.1
